TPU v7x, 32 devices: a whole 2x2x4 slice. The times are simulated.
32 devices in a mesh: fs: 16 (over z, y, x), tp: 2 (over core).
Axes of the slice: x: 2, y: 2, z: 4, core: 2. Of those that a mesh axis runs over, the one named last changes fastest.
Arguments:
- tokens: bfloat16 [12288, 2048], P('fs'), may hold values from -6 to 6
- norm_gain: float32 [2048], replicated, may hold values from 0.1 to 1.9
- gate_weight: float32 [2048, 5632], P('fs', 'tp'), may hold values from -0.125 to 0.125
- up_weight: float32 [2048, 5632], P('fs', 'tp'), may hold values from -0.125 to 0.125
- gate_scale: float32 [5632], P('tp'), may hold values from 0.1 to 1.9
- up_scale: float32 [5632], P('tp'), may hold values from 0.1 to 1.9
- down_weight: float32 [5632, 2048], P('tp', 'fs'), may hold values from -0.078125 to 0.078125
- down_scale: float32 [2048], P('tp'), may hold values from 0.1 to 1.9
Outputs:
- mixed: bfloat16 [12288, 2048], P('fs', 'tp')
All inputs are finite; a program needn't handle non-finite values.
Results may differ from a plain program's by a relative error of at most 0.014.
Values may be sent and summed in bfloat16 or wider, within the bound.
A program may use at most 128 MiB of HBM per device.

v0:
```python
import jax
import jax.numpy as jnp
from jax import lax
from jax.sharding import PartitionSpec as P


def body(tokens, norm_gain, gate_weight, up_weight, gate_scale, up_scale, down_weight, down_scale):
    values = tokens.astype(jnp.float32)
    normed = (
        values * lax.rsqrt(jnp.mean(values * values, axis=-1, keepdims=True) + 1e-06) * norm_gain
    ).astype(jnp.bfloat16)
    gate_low = gate_weight.astype(jnp.bfloat16)
    up_low = up_weight.astype(jnp.bfloat16)
    down_low = down_weight.astype(jnp.bfloat16)

    def add_rows(piece):
        return jnp.dot(normed, piece, preferred_element_type=jnp.float32)

    gate = add_rows(lax.all_gather(gate_low, "fs", axis=0, tiled=True))
    up = add_rows(lax.all_gather(up_low, "fs", axis=0, tiled=True))
    hidden = (jax.nn.silu(gate * gate_scale) * (up * up_scale)).astype(jnp.bfloat16)
    terms = jnp.dot(
        hidden,
        lax.all_gather(down_low, "fs", axis=1, tiled=True),
        preferred_element_type=jnp.float32,
    )
    summed = lax.psum_scatter(
        terms.astype(jnp.bfloat16), "tp", scatter_dimension=1, tiled=True
    ).astype(jnp.float32)
    return (summed * down_scale).astype(jnp.bfloat16)


def solution(mesh):
    in_specs = (
        P("fs", None),
        P(),
        P("fs", "tp"),
        P("fs", "tp"),
        P("tp"),
        P("tp"),
        P("tp", "fs"),
        P("tp"),
    )
    out_specs = P("fs", "tp")
    return jax.shard_map(body, mesh=mesh, in_specs=in_specs, out_specs=out_specs, check_vma=False)
```

profile of v0, /device:TPU:1, one launch (start us, length us, event | category | flops | bytes accessed | tf_op | source)
XLA Modules:
  0.0 527.3 jit_solution(15337581504936662027)
XLA Ops:
  6.5 0.0 copy-start
  6.5 0.0 copy-start.4
  6.5 0.0 all-gather.4.cloned.1.call-start
  6.5 2.5 convert_element_type.29
  9.0 0.0 all-gather.4.cloned.1.call-update
  9.0 0.0 all-gather.6.cloned.1.call-start
  9.1 2.3 convert_element_type.30
  11.4 0.0 all-gather.6.cloned.1.call-update
  11.4 0.0 all-gather.8.cloned.1.call-start
  11.5 2.3 convert_element_type.32
  13.8 0.0 all-gather.8.cloned.1.call-update
  13.8 0.0 reduce-scatter.2.cloned.1.call-start
  13.8 0.0 copy-done
  13.8 0.7 fusion
  14.5 0.0 copy-start.2
  14.6 0.0 copy-start.3
  14.6 138.1 %all-gather.4.cloned.1.call-done = bf16[2048,2816]{1,0:T(8,128)(2,1)} async-done(((bf16[128,2816]{1,0:T(8,128)(2,1)}), bf16[2048,2816]{1,0:T(8,128)(2,1)}) %all-gather.4.cloned.1.call-update) | async-done | bytes 11534352 | tf_op jit(solution)/shard_map/all_gather | solution.py:19
  152.7 0.0 copy-done.4
  152.7 14.9 %fusion.9 = f32[768,2816]{1,0:T(8,128)} fusion(bf16[2048,2816]{1,0:T(8,128)(2,1)} %all-gather.4.cloned.1.call-done, bf16[768,2048]{1,0:T(8,128)(2,1)S(1)} %copy-done, f32[2048]{0:T(1024)S(1)} %copy-done.4, f32[768]{0:T(1024)S(1)} %add_rsqrt_fusion), kind=kOutput, calls=%fused_computation.11 | convolution fusion | flops 8864661504 | bytes 23342080 | tf_op jit(solution)/shard_map/dot_general | solution.py:17
  167.6 0.0 copy-start.1
  167.6 127.5 %all-gather.6.cloned.1.call-done = bf16[2048,2816]{1,0:T(8,128)(2,1)} async-done(((bf16[128,2816]{1,0:T(8,128)(2,1)}), bf16[2048,2816]{1,0:T(8,128)(2,1)}) %all-gather.6.cloned.1.call-update) | async-done | bytes 11534352 | tf_op jit(solution)/shard_map/all_gather | solution.py:20
  295.1 183.2 %all-gather.8.cloned.1.call-done = bf16[2816,2048]{1,0:T(8,128)(2,1)} async-done(((bf16[2816,128]{1,0:T(8,128)(2,1)}), bf16[2816,2048]{1,0:T(8,128)(2,1)}) %all-gather.8.cloned.1.call-update) | async-done | bytes 11534352 | tf_op jit(solution)/shard_map/all_gather | solution.py:24
  478.2 0.0 copy-done.2
  478.2 0.0 copy-done.3
  478.2 29.0 %fusion.6 = bf16[768,2048]{1,0:T(8,128)(2,1)} fusion(bf16[2816,2048]{1,0:T(8,128)(2,1)} %all-gather.8.cloned.1.call-done, f32[768,2816]{1,0:T(8,128)} %fusion.9, bf16[2048,2816]{1,0:T(8,128)(2,1)} %all-gather.6.cloned.1.call-done, f32[2816]{0:T(1024)S(1)} %copy-done.2, f32[2816]{0:T(1024)S(1)} %copy-done.3, bf16[768,2048]{1,0:T(8,128)(2,1)S(1)} %copy-done, ...), kind=kOutput, calls=%fused_computation.9 | convolution fusion | flops 17741905920 | bytes 38044672 | tf_op jit(solution)/shard_map/dot_general | solution.py:22
  507.2 0.0 reduce-scatter.2.cloned.1.call-update
  507.3 10.5 %reduce-scatter.2.cloned.1.call-done = bf16[768,1024]{1,0:T(8,128)(2,1)} async-done(((bf16[768,2048]{1,0:T(8,128)(2,1)}), bf16[768,1024]{1,0:T(8,128)(2,1)}) %reduce-scatter.2.cloned.1.call-update) | async-done | bytes 1572880 | tf_op jit(solution)/shard_map/reduce_scatter | solution.py:27
  517.8 0.0 copy-done.1
  517.8 3.0 multiply_convert_fusion.1
  (1 shorter events, 0.0 us)
Async XLA Ops:
  6.5 7.3 %copy-start = (bf16[768,2048]{1,0:T(8,128)(2,1)S(1)}, bf16[768,2048]{1,0:T(8,128)(2,1)}, u32[]{:S(2)}) copy-start(bf16[768,2048]{1,0:T(8,128)(2,1)} %param.8) | copy-start | bytes 9437188
  6.5 146.2 %copy-start.4 = (f32[2048]{0:T(1024)S(1)}, f32[2048]{0:T(1024)}, u32[]{:S(2)}) copy-start(f32[2048]{0:T(1024)} %param.9) | copy-start | bytes 24580
  6.5 146.2 %all-gather.4.cloned.1.call-start = ((), (), s32[]{:S(2)}) async-start(), calls=%async_computation.1 | async-start | bytes 12255232 | tf_op jit(solution)/shard_map/all_gather | solution.py:19
  9.0 286.1 %all-gather.6.cloned.1.call-start = ((), (), s32[]{:S(2)}) async-start(), calls=%async_computation.2 | async-start | bytes 12255232 | tf_op jit(solution)/shard_map/all_gather | solution.py:20
  11.4 466.8 %all-gather.8.cloned.1.call-start = ((), (), s32[]{:S(2)}) async-start(), calls=%async_computation.3 | async-start | bytes 12255232 | tf_op jit(solution)/shard_map/all_gather | solution.py:24
  13.8 504.0 %reduce-scatter.2.cloned.1.call-start = ((), (), s32[]{:S(2)}) async-start(), calls=%async_computation.4 | async-start | bytes 4718592 | tf_op jit(solution)/shard_map/reduce_scatter | solution.py:27
  14.5 463.7 %copy-start.2 = (f32[2816]{0:T(1024)S(1)}, f32[2816]{0:T(1024)}, u32[]{:S(2)}) copy-start(f32[2816]{0:T(1024)} %param.13) | copy-start | bytes 33796
  14.6 463.7 %copy-start.3 = (f32[2816]{0:T(1024)S(1)}, f32[2816]{0:T(1024)}, u32[]{:S(2)}) copy-start(f32[2816]{0:T(1024)} %param.12) | copy-start | bytes 33796
  167.6 350.2 %copy-start.1 = (f32[1024]{0:T(1024)S(1)}, f32[1024]{0:T(1024)}, u32[]{:S(2)}) copy-start(f32[1024]{0:T(1024)} %param.15) | copy-start | bytes 12292
Sparse Core Ops, SparseCore 0:
  10.1 142.5 all-gather.3
  155.4 139.5 all-gather.5
  297.8 180.3 all-gather.7
  507.4 10.3 reduce-scatter.1
where the time goes:
time: 528 us; the launch traced here: 527 us
  waiting for transfers between devices  459 us (87%)
  matrix products  43.9 us (8%)
  between operations  13.2 us (2%)
  other arithmetic  10.7 us (2%)
    all_gather x1, waiting for transfers between devices, body(): lax.all_gather(down_low, 'fs', axis=1, tiled=True)  183 us
    all_gather x1, waiting for transfers between devices, body(): gate = add_rows(lax.all_gather(gate_low, 'fs', axis=0, tiled=True))  138 us
    all_gather x1, waiting for transfers between devices, body(): up = add_rows(lax.all_gather(up_low, 'fs', axis=0, tiled=True))  128 us
    dot_general x1, matrix products, body(): jnp.dot(hidden, lax.all_gather(down_low, 'fs', axis=1, tiled=True), prefe...  29 us
    dot_general x1, matrix products, add_rows(): return jnp.dot(normed, piece, preferred_element_type=jnp.float32)  14.9 us
  transfers between devices with their start and end apart: 4, of which 4 were waited for; matrix products, arithmetic and copies ran while one was open for 4% of the time, Pallas kernels for 0%

commit v1 on v0

v1 whole, which is shorter than its diff:
```python
import jax
import jax.numpy as jnp
from jax import lax
from jax.experimental import pallas as pl
from jax.experimental.pallas import tpu as pltpu
from jax.sharding import PartitionSpec as P

MESH = pl.DeviceIdType.MESH
NT = (((1,), (1,)), ((), ()))
NN = (((1,), (0,)), ((), ()))


def norm(tokens, norm_gain):
    values = tokens.astype(jnp.float32)
    return (
        values * lax.rsqrt(jnp.mean(values * values, axis=-1, keepdims=True) + 1e-06) * norm_gain
    ).astype(jnp.bfloat16)


def gathered(tokens, norm_gain, gate_weight, up_weight, gate_scale, up_scale, down_weight, down_scale):
    normed = norm(tokens, norm_gain)

    def add_rows(piece):
        return jnp.dot(normed, piece, preferred_element_type=jnp.float32)

    gate = add_rows(lax.all_gather(gate_weight.astype(jnp.bfloat16), "fs", axis=0, tiled=True))
    up = add_rows(lax.all_gather(up_weight.astype(jnp.bfloat16), "fs", axis=0, tiled=True))
    hidden = (jax.nn.silu(gate * gate_scale) * (up * up_scale)).astype(jnp.bfloat16)
    terms = jnp.dot(
        hidden,
        lax.all_gather(down_weight.astype(jnp.bfloat16), "fs", axis=1, tiled=True),
        preferred_element_type=jnp.float32,
    )
    summed = lax.psum_scatter(
        terms.astype(jnp.bfloat16), "tp", scatter_dimension=1, tiled=True
    ).astype(jnp.float32)
    return (summed * down_scale).astype(jnp.bfloat16)


def kernel(
    gu_ref, d_ref, xn_ref, gs_ref, us_ref, ds_ref, out_ref,
    xbuf, wgu, wd, accg, accu, hid, pbuf, rbuf,
    lw_sem, lx_sem, rsh_send, rsh_recv, x_send, x_recv, xf_send, xf_recv,
    z_send, z_recv, p_send, p_recv, r_send, r_recv,
):
    f, c = lax.axis_index("fs"), lax.axis_index("tp")
    z, q = lax.div(f, 4), lax.rem(f, 4)
    qk = [q, q + 1 - 2 * lax.rem(q, 2), lax.rem(q + 2, 4), 3 - q]
    part = wd.shape[1]
    width = 4 * wd.shape[2]
    rows = xn_ref.shape[0]
    half = rows // 2
    tile = rows // 3
    tiles = rows // tile
    partner = (f, 1 - c)

    def at(k):
        return (4 * z + qk[k], c)

    def rcopy(src, dst, ssem, rsem, dev):
        return pltpu.make_async_remote_copy(
            src_ref=src, dst_ref=dst, send_sem=ssem, recv_sem=rsem,
            device_id=dev, device_id_type=MESH,
        )

    barrier = pltpu.get_barrier_semaphore()

    def greet(dev):
        pl.semaphore_signal(barrier, inc=1, device_id=dev, device_id_type=MESH)

    greet(partner)
    for k in (1, 2, 3):
        greet(at(k))
    pl.when(z > 0)(lambda: greet((f - 4, c)))
    pl.when(z < 3)(lambda: greet((f + 4, c)))

    slot = [wgu, wd]

    def stored(cls, k):
        cut = pl.ds(pl.multiple_of(qk[k] * part, 16), part)
        return gu_ref.at[:, cut, :] if cls == 0 else d_ref.at[cut, :]

    def own(cls):
        return pltpu.make_async_copy(stored(cls, 0), slot[cls].at[f], lw_sem.at[cls])

    def rsh(cls, k, landing):
        return rcopy(
            stored(cls, k), slot[cls].at[landing],
            rsh_send.at[cls, k - 1], rsh_recv.at[cls, k - 1], at(k),
        )

    mine = pl.ds(pl.multiple_of(half * c, 16), half)
    theirs = pl.ds(pl.multiple_of(half * (1 - c), 16), half)

    def xcopy(k, landing):
        return rcopy(
            xn_ref.at[mine, :], xbuf.at[landing, mine, :],
            x_send.at[k - 1], x_recv.at[k - 1], at(k),
        )

    def xshare(k, cut):
        return rcopy(
            xbuf.at[qk[k], mine, :], xbuf.at[qk[k], cut, :],
            xf_send.at[k - 1], xf_recv.at[k - 1], partner,
        )

    local_x = pltpu.make_async_copy(xn_ref, xbuf.at[q], lx_sem)

    def zcopy(cls, i, d):
        dev = (f + 4, c) if d == 0 else (f - 4, c)
        return rcopy(slot[cls].at[i], slot[cls].at[i], z_send.at[d, cls, i], z_recv.at[cls, i], dev)

    def up_down(cls, i):
        pl.when(z < 3)(lambda: zcopy(cls, i, 0).start())
        pl.when(z > 0)(lambda: zcopy(cls, i, 1).start())

    def relay(cls, r):
        for k in range(4):
            low = 4 * (z - r) + qk[k]
            high = 4 * (z + r) + qk[k]

            @pl.when(z >= r)
            def _():
                zcopy(cls, low, 0).wait_recv()
                if r < 3:
                    pl.when(z < 3)(lambda: zcopy(cls, low, 0).start())

            @pl.when(z + r <= 3)
            def _():
                zcopy(cls, high, 1).wait_recv()
                if r < 3:
                    pl.when(z > 0)(lambda: zcopy(cls, high, 1).start())

    own(0).start()
    own(1).start()
    local_x.start()
    pl.semaphore_wait(barrier, 4 + jnp.minimum(z, 1) + jnp.minimum(3 - z, 1))

    for cls in (0, 1):
        for k in (1, 2, 3):
            rsh(cls, k, f).start()
    for k in (1, 2, 3):
        xcopy(k, q).start()
    own(0).wait()
    up_down(0, f)
    for k in (1, 2, 3):
        rsh(0, k, 4 * z + qk[k]).wait_recv()
        up_down(0, 4 * z + qk[k])
    relay(0, 1)
    relay(0, 2)
    own(1).wait()
    up_down(1, f)
    for k in (1, 2, 3):
        rsh(1, k, 4 * z + qk[k]).wait_recv()
        up_down(1, 4 * z + qk[k])
    for k in (1, 2, 3):
        xcopy(k, qk[k]).wait_recv()
        xshare(k, mine).start()
    local_x.wait()
    relay(1, 1)
    for k in (1, 2, 3):
        xshare(k, theirs).wait_recv()

    side = lax.div(z, 2)
    zz = z + side * (3 - 2 * z)

    def turn(t):
        base = t if t >= 2 else lax.rem(t + zz, 2)
        return base + side * (3 - 2 * base)

    def columns(s):
        return pl.ds(pl.multiple_of(s * width, 128), width)

    def gate_up(t):
        s = turn(t)

        def step(m, _):
            there = pl.ds(pl.multiple_of(lax.rem(m, tiles) * tile, 16), tile)
            here = pl.ds(pl.multiple_of(m * tile, 16), tile)
            x = xbuf[lax.div(m, tiles), there, columns(s)]
            found = []
            for j, acc in enumerate((accg, accu)):
                w = jnp.concatenate([wgu[4 * s + k, j] for k in range(4)], axis=1)
                part_sum = lax.dot_general(x, w, NT, preferred_element_type=jnp.float32)
                if t > 0:
                    part_sum = part_sum + acc[here, :]
                if t < 3:
                    acc[here, :] = part_sum
                found.append(part_sum)
            if t == 3:
                g = found[0] * gs_ref[...]
                u = found[1] * us_ref[...]
                hid[here, :] = (g / (1.0 + jnp.exp(-g)) * u).astype(jnp.bfloat16)
            return 0

        lax.fori_loop(0, 4 * tiles, step, 0)

    gate_up(0)
    gate_up(1)
    relay(1, 2)
    gate_up(2)
    relay(0, 3)
    gate_up(3)
    for k in (1, 2, 3):
        xshare(k, mine).wait_send()

    order = (3, 1, 2, 0)

    def pcopy(s, k):
        i = lax.rem(s, 2)
        return rcopy(
            xbuf.at[qk[k], :, columns(s)], pbuf.at[i, qk[k]],
            p_send.at[i, qk[k]], p_recv.at[i, qk[k]], partner,
        )

    def scopy(s, k):
        i = lax.rem(s, 2)
        return rcopy(
            xbuf.at[qk[k], :, columns(s)], rbuf.at[i, k - 1],
            r_send.at[i, k - 1], r_recv.at[i, k - 1], at(k),
        )

    def finish(s, k):
        @pl.when(lax.div(s, 2) == c)
        def _():
            pcopy(s, k).wait_recv()

            def step(m, _):
                here = pl.ds(pl.multiple_of(m * tile, 16), tile)
                both = xbuf[qk[k], here, columns(s)].astype(jnp.float32) + pbuf[
                    lax.rem(s, 2), qk[k], here, :
                ].astype(jnp.float32)
                xbuf[qk[k], here, columns(s)] = both.astype(jnp.bfloat16)
                return 0

            lax.fori_loop(0, tiles, step, 0)
            if k:
                scopy(s, k).start()

    def down(t):
        s = turn(t)
        for n, k in enumerate(order):
            def step(m, _):
                here = pl.ds(pl.multiple_of(m * tile, 16), tile)
                h = hid[pl.ds(pl.multiple_of(qk[k] * rows + m * tile, 16), tile), :]
                w = jnp.concatenate([wd[4 * s + j] for j in range(4)], axis=1)
                o = lax.dot_general(h, w, NN, preferred_element_type=jnp.float32)
                xbuf[qk[k], here, columns(s)] = o.astype(jnp.bfloat16)
                return 0

            lax.fori_loop(0, tiles, step, 0)
            pl.when(lax.div(s, 2) != c)(lambda: pcopy(s, k).start())
            if n:
                finish(s, order[n - 1])
        finish(s, order[-1])

    down(0)
    down(1)
    down(2)
    relay(1, 3)
    down(3)

    for i in range(2):
        s = 2 * c + i
        for k in (1, 2, 3):
            scopy(s, k).wait_recv()

        def step(m, _):
            here = pl.ds(pl.multiple_of(m * tile, 16), tile)
            total = xbuf[q, here, columns(s)].astype(jnp.float32)
            for k in range(3):
                total = total + rbuf[i, k, here, :].astype(jnp.float32)
            cols = slice(i * width, (i + 1) * width)
            out_ref[here, cols] = (total * ds_ref[:, cols]).astype(jnp.bfloat16)
            return 0

        lax.fori_loop(0, tiles, step, 0)

    for cls in (0, 1):
        for k in (1, 2, 3):
            rsh(cls, k, f).wait_send()
        for r in range(3):
            for k in range(4):
                low, high = 4 * (z - r) + qk[k], 4 * (z + r) + qk[k]
                pl.when((z >= r) & (z < 3))(lambda: zcopy(cls, low, 0).wait_send())
                pl.when((z + r <= 3) & (z > 0))(lambda: zcopy(cls, high, 1).wait_send())
    for k in (1, 2, 3):
        xcopy(k, q).wait_send()
    for i in range(2):
        for k in range(4):
            pcopy(2 * (1 - c) + i, k).wait_send()
            if k:
                scopy(2 * c + i, k).wait_send()


def planes(tokens, norm_gain, gate_weight, up_weight, gate_scale, up_scale, down_weight, down_scale):
    rows, model = tokens.shape
    block, units = gate_weight.shape
    part, width = units // 4, 4 * block
    normed = norm(tokens, norm_gain)
    gu = jnp.stack([gate_weight.astype(jnp.bfloat16).T, up_weight.astype(jnp.bfloat16).T])
    low = down_weight.astype(jnp.bfloat16)
    first = lax.rem(lax.axis_index("fs"), 4) * part
    gs = lax.dynamic_slice(gate_scale, (first,), (part,))[None]
    us = lax.dynamic_slice(up_scale, (first,), (part,))[None]
    bf, f32, dma = jnp.bfloat16, jnp.float32, pltpu.SemaphoreType.DMA
    hbm = pl.BlockSpec(memory_space=pl.ANY)
    vmem = pl.BlockSpec(memory_space=pltpu.VMEM)
    return pl.pallas_call(
        kernel,
        out_shape=jax.ShapeDtypeStruct((rows, down_scale.shape[0]), bf),
        in_specs=[hbm, hbm, hbm, vmem, vmem, vmem],
        out_specs=vmem,
        scratch_shapes=[
            pltpu.VMEM((4, rows, model), bf),
            pltpu.VMEM((16, 2, part, block), bf),
            pltpu.VMEM((16, part, block), bf),
            pltpu.VMEM((4 * rows, part), f32),
            pltpu.VMEM((4 * rows, part), f32),
            pltpu.VMEM((4 * rows, part), bf),
            pltpu.VMEM((2, 4, rows, width), bf),
            pltpu.VMEM((2, 3, rows, width), bf),
            dma((2,)), dma, dma((2, 3)), dma((2, 3)),
            dma((3,)), dma((3,)), dma((3,)), dma((3,)),
            dma((2, 2, 16)), dma((2, 16)),
            dma((2, 4)), dma((2, 4)), dma((2, 3)), dma((2, 3)),
        ],
        compiler_params=pltpu.CompilerParams(
            collective_id=0, has_side_effects=True, vmem_limit_bytes=67043328
        ),
    )(gu, low, normed, gs, us, down_scale[None])


def solution(mesh):
    in_specs = (
        P("fs", None),
        P(),
        P("fs", "tp"),
        P("fs", "tp"),
        P("tp"),
        P("tp"),
        P("tp", "fs"),
        P("tp"),
    )
    out_specs = P("fs", "tp")
    body = planes if (mesh.shape["fs"], mesh.shape["tp"]) == (16, 2) else gathered
    return jax.shard_map(body, mesh=mesh, in_specs=in_specs, out_specs=out_specs, check_vma=False)
```

time: 528 us -> 242 us (0.46)
  waiting for transfers between devices: 459 us -> 0 us
  Pallas kernels: 0 us -> 224 us
  matrix products: 43.9 us -> 0 us
  between operations: 13.2 us -> 0.03 us
  local copies, waits for them, and re-layouts: 0.02 us -> 9.29 us
    all_gather x3 -> x0, waiting for transfers between devices: 449 us -> none  [the longest x1 183 us: body(): lax.all_gather(down_low, 'fs', axis=1, tiled=True)]
    pallas_call x0 -> x1, Pallas kernels: none -> 224 us  [planes(): pl.pallas_call(kernel, out_shape=jax.ShapeDtypeStruct((rows, down_scale.s...]
    dot_general x2 -> x0, matrix products: 43.9 us -> none  [the longest x1 29 us: body(): jnp.dot(hidden, lax.all_gather(down_low, 'fs', axis=1, tiled=True), prefe...]
    reduce_scatter x1 -> x0, waiting for transfers between devices: 10.5 us -> none  [body(): lax.psum_scatter(terms.astype(jnp.bfloat16), 'tp', scatter_dimension=1, t...]
    convert_element_type x4 -> x2, other arithmetic: 10 us -> 3.38 us  [the longest x1 2.44 us: norm(): return (values * lax.rsqrt(jnp.mean(values * values, axis=-1, keepdims=Tr...]
    unnamed x10 -> x11, local copies, waits for them, and re-layouts: 0.02 us -> 6.47 us
  transfers between devices with their start and end apart: 4 -> 0, of which waited for: 4 -> 0; matrix products, arithmetic and copies ran while one was open for 4% -> 0% of each run, Pallas kernels for 0% -> 0%
where the time goes in v1:
time: 242 us
  Pallas kernels  224 us (93%)
  local copies, waits for them, and re-layouts  9.29 us (4%)
  other arithmetic  8.63 us (4%)
    pallas_call x1, Pallas kernels, planes(): pl.pallas_call(kernel, out_shape=jax.ShapeDtypeStruct((rows, down_scale.s...  224 us
    unnamed x11, local copies, waits for them, and re-layouts  6.47 us

profile of v1, /device:TPU:1, one launch (start us, length us, event | category | flops | bytes accessed | tf_op | source)
XLA Modules:
  0.0 241.7 jit_solution(18257722815815014564)
XLA Ops:
  0.0 0.0 copy-start.1
  0.0 0.9 dynamic_slice.6
  0.9 0.6 broadcast_in_dim.11.gs_ref
  1.5 0.8 dynamic_slice.7
  2.3 0.6 broadcast_in_dim.12.us_ref
  2.8 2.6 %fusion = f32[768]{0:T(1024)S(1)} fusion(bf16[768,2048]{1,0:T(8,128)(2,1)} %param.8), kind=kLoop, calls=%fused_computation.2 | loop fusion | flops 4717824 | bytes 3148800 | tf_op jit(solution)/shard_map/reduce_sum | solution.py:16
  5.4 0.0 copy-done.1
  5.4 1.1 copy.9
  6.6 0.0 copy-start
  6.6 0.0 copy-start.3
  6.6 2.6 %copy.10 = bf16[128,2816]{0,1:T(8,128)(2,1)} copy(f32[128,2816]{1,0:T(8,128)} %param.11) | data formatting | bytes 2162688 | tf_op args[3]
  9.2 0.0 copy-start.2
  9.2 2.7 %pad_maximum_fusion.gu_ref = bf16[2,2816,128]{2,1,0:T(8,128)(2,1)} fusion(bf16[1,2816,128]{2,1,0:T(8,128)(2,1)} %bitcast.12, bf16[1,2816,128]{2,1,0:T(8,128)(2,1)} %bitcast.11), kind=kLoop, calls=%fused_computation.5 | loop fusion | flops 720896 | bytes 2883584 | tf_op jit(solution)/shard_map/stack | solution.py:301
  11.9 0.0 copy-done.2
  11.9 0.9 convert_element_type.17.d_ref
  12.8 0.0 copy-done
  12.8 0.0 copy-done.3
  12.8 2.4 %fusion.2.xn_ref = bf16[768,2048]{1,0:T(8,128)(2,1)} fusion(bf16[768,2048]{1,0:T(8,128)(2,1)S(1)} %copy-done, f32[2048]{0:T(1024)S(1)} %copy-done.3, f32[768]{0:T(1024)S(1)} %add_rsqrt_fusion), kind=kLoop, calls=%fused_computation.4 | loop fusion | flops 6291456 | bytes 6302720 | tf_op jit(solution)/shard_map/convert_element_type | solution.py:17
  15.3 223.8 %shard_map.82 = bf16[768,1024]{1,0:T(8,128)(2,1)} custom-call(bf16[2,2816,128]{2,1,0:T(8,128)(2,1)} %pad_maximum_fusion.gu_ref, bf16[2816,128]{1,0:T(8,128)(2,1)} %convert_element_type.17.d_ref, bf16[768,2048]{1,0:T(8,128)(2,1)} %fusion.2.xn_ref, f32[1,704]{1,0:T(1,128)} %broadcast_in_dim.11.gs_ref, f32[1,704]{1,0:T(1,128)} %broadcast_in_dim.12.us_ref, ...), custom_call_target="tpu_custom_call" | custom-call | tf_op jit(solution)/shard_map/pallas_call | solution.py:309
  239.1 2.7 %copy.12 = bf16[768,1024]{1,0:T(8,128)(2,1)} copy(bf16[768,1024]{1,0:T(8,128)(2,1)} %shard_map.82) | data formatting | bytes 3145728
  (1 shorter events, 0.0 us)
Async XLA Ops:
  0.0 5.4 %copy-start.1 = (f32[128,2816]{1,0:T(8,128)S(1)}, f32[128,2816]{1,0:T(8,128)}, u32[]{:S(2)}) copy-start(f32[128,2816]{1,0:T(8,128)} %param.10) | copy-start | bytes 4325380
  6.6 6.3 %copy-start = (bf16[768,2048]{1,0:T(8,128)(2,1)S(1)}, bf16[768,2048]{1,0:T(8,128)(2,1)}, u32[]{:S(2)}) copy-start(bf16[768,2048]{1,0:T(8,128)(2,1)} %param.8) | copy-start | bytes 9437188
  6.6 6.3 %copy-start.3 = (f32[2048]{0:T(1024)S(1)}, f32[2048]{0:T(1024)}, u32[]{:S(2)}) copy-start(f32[2048]{0:T(1024)} %param.9) | copy-start | bytes 24580
  9.2 2.7 %copy-start.2 = (f32[2816,128]{1,0:T(8,128)S(1)}, f32[2816,128]{1,0:T(8,128)}, u32[]{:S(2)}) copy-start(f32[2816,128]{1,0:T(8,128)} %param.14) | copy-start | bytes 4325380

commit v2 on v1

--- a/solution.py
+++ b/solution.py
@@ -40,7 +40,7 @@
 def kernel(
     gu_ref, d_ref, xn_ref, gs_ref, us_ref, ds_ref, out_ref,
     xbuf, wgu, wd, accg, accu, hid, pbuf, rbuf,
-    lw_sem, lx_sem, rsh_send, rsh_recv, x_send, x_recv, xf_send, xf_recv,
+    lw_sem, lx_sem, rsh_send, rsh_recv, x_send, x_recv, f_send, f_recv, xf_send, xf_recv,
     z_send, z_recv, p_send, p_recv, r_send, r_recv,
 ):
     f, c = lax.axis_index("fs"), lax.axis_index("tp")
@@ -50,6 +50,7 @@
     width = 4 * wd.shape[2]
     rows = xn_ref.shape[0]
     half = rows // 2
+    quarter = half // 2
     tile = rows // 3
     tiles = rows // tile
     partner = (f, 1 - c)
@@ -77,8 +78,8 @@
     slot = [wgu, wd]
 
     def stored(cls, k):
-        cut = pl.ds(pl.multiple_of(qk[k] * part, 16), part)
-        return gu_ref.at[:, cut, :] if cls == 0 else d_ref.at[cut, :]
+        units = pl.ds(pl.multiple_of(qk[k] * part, 16), part)
+        return gu_ref.at[:, units, :] if cls == 0 else d_ref.at[units, :]
 
     def own(cls):
         return pltpu.make_async_copy(stored(cls, 0), slot[cls].at[f], lw_sem.at[cls])
@@ -89,19 +90,25 @@
             rsh_send.at[cls, k - 1], rsh_recv.at[cls, k - 1], at(k),
         )
 
-    mine = pl.ds(pl.multiple_of(half * c, 16), half)
-    theirs = pl.ds(pl.multiple_of(half * (1 - c), 16), half)
-
-    def xcopy(k, landing):
-        return rcopy(
-            xn_ref.at[mine, :], xbuf.at[landing, mine, :],
-            x_send.at[k - 1], x_recv.at[k - 1], at(k),
-        )
-
-    def xshare(k, cut):
-        return rcopy(
-            xbuf.at[qk[k], mine, :], xbuf.at[qk[k], cut, :],
-            xf_send.at[k - 1], xf_recv.at[k - 1], partner,
+    def cut(core, p):
+        return pl.ds(pl.multiple_of(half * core + quarter * p, 16), quarter)
+
+    def xcopy(k, p, landing):
+        return rcopy(
+            xn_ref.at[cut(c, p), :], xbuf.at[landing, cut(c, p), :],
+            x_send.at[k - 1, p], x_recv.at[k - 1, p], at(k),
+        )
+
+    def fcopy(p, k):
+        return rcopy(
+            xbuf.at[qk[k], cut(c, p), :], xbuf.at[qk[k], cut(c, p), :],
+            f_send.at[p], f_recv.at[p], at(2 - p),
+        )
+
+    def xshare(k, p, core):
+        return rcopy(
+            xbuf.at[qk[k], cut(core, p), :], xbuf.at[qk[k], cut(core, p), :],
+            xf_send.at[k - 1, p], xf_recv.at[k - 1, p], partner,
         )
 
     local_x = pltpu.make_async_copy(xn_ref, xbuf.at[q], lx_sem)
@@ -139,27 +146,35 @@
     for cls in (0, 1):
         for k in (1, 2, 3):
             rsh(cls, k, f).start()
-    for k in (1, 2, 3):
-        xcopy(k, q).start()
+    for k, p in ((1, 0), (2, 1), (1, 1), (2, 0)):
+        xcopy(k, p, q).start()
     own(0).wait()
     up_down(0, f)
     for k in (1, 2, 3):
         rsh(0, k, 4 * z + qk[k]).wait_recv()
         up_down(0, 4 * z + qk[k])
     relay(0, 1)
+    for p in (0, 1):
+        xcopy(1 + p, p, qk[1 + p]).wait_recv()
+        fcopy(p, 1 + p).start()
+        xshare(1 + p, p, c).start()
     relay(0, 2)
     own(1).wait()
     up_down(1, f)
     for k in (1, 2, 3):
         rsh(1, k, 4 * z + qk[k]).wait_recv()
         up_down(1, 4 * z + qk[k])
-    for k in (1, 2, 3):
-        xcopy(k, qk[k]).wait_recv()
-        xshare(k, mine).start()
+    for p in (0, 1):
+        xcopy(2 - p, p, qk[2 - p]).wait_recv()
+        xshare(2 - p, p, c).start()
     local_x.wait()
     relay(1, 1)
+    for p in (0, 1):
+        fcopy(p, 3).wait_recv()
+        xshare(3, p, c).start()
     for k in (1, 2, 3):
-        xshare(k, theirs).wait_recv()
+        for p in (0, 1):
+            xshare(k, p, 1 - c).wait_recv()
 
     side = lax.div(z, 2)
     zz = z + side * (3 - 2 * z)
@@ -201,8 +216,10 @@
     gate_up(2)
     relay(0, 3)
     gate_up(3)
-    for k in (1, 2, 3):
-        xshare(k, mine).wait_send()
+    for p in (0, 1):
+        fcopy(p, 1 + p).wait_send()
+        for k in (1, 2, 3):
+            xshare(k, p, c).wait_send()
 
     order = (3, 1, 2, 0)
 
@@ -284,8 +301,9 @@
                 low, high = 4 * (z - r) + qk[k], 4 * (z + r) + qk[k]
                 pl.when((z >= r) & (z < 3))(lambda: zcopy(cls, low, 0).wait_send())
                 pl.when((z + r <= 3) & (z > 0))(lambda: zcopy(cls, high, 1).wait_send())
-    for k in (1, 2, 3):
-        xcopy(k, q).wait_send()
+    for k in (1, 2):
+        for p in (0, 1):
+            xcopy(k, p, q).wait_send()
     for i in range(2):
         for k in range(4):
             pcopy(2 * (1 - c) + i, k).wait_send()
@@ -321,7 +339,7 @@
             pltpu.VMEM((2, 4, rows, width), bf),
             pltpu.VMEM((2, 3, rows, width), bf),
             dma((2,)), dma, dma((2, 3)), dma((2, 3)),
-            dma((3,)), dma((3,)), dma((3,)), dma((3,)),
+            dma((2, 2)), dma((2, 2)), dma((2,)), dma((2,)), dma((3, 2)), dma((3, 2)),
             dma((2, 2, 16)), dma((2, 16)),
             dma((2, 4)), dma((2, 4)), dma((2, 3)), dma((2, 3)),
         ],

time: 242 us -> 245 us (1.012)
  Pallas kernels: 224 us -> 227 us
    pallas_call x1, Pallas kernels: 224 us -> 227 us  [planes(): pl.pallas_call(kernel, out_shape=jax.ShapeDtypeStruct((rows, down_scale.s...]
where the time goes in v2:
time: 245 us
  Pallas kernels  227 us (93%)
  local copies, waits for them, and re-layouts  9.29 us (4%)
  other arithmetic  8.63 us (4%)
    pallas_call x1, Pallas kernels, planes(): pl.pallas_call(kernel, out_shape=jax.ShapeDtypeStruct((rows, down_scale.s...  227 us
    unnamed x11, local copies, waits for them, and re-layouts  6.47 us

profile of v2, /device:TPU:1, one launch (start us, length us, event | category | flops | bytes accessed | tf_op | source)
XLA Modules:
  0.0 245.1 jit_solution(14205497800193570846)
XLA Ops:
  0.0 0.0 copy-start.1
  0.0 0.9 dynamic_slice.6
  0.9 0.6 broadcast_in_dim.11.gs_ref
  1.5 0.8 dynamic_slice.7
  2.3 0.6 broadcast_in_dim.12.us_ref
  2.8 2.6 %fusion = f32[768]{0:T(1024)S(1)} fusion(bf16[768,2048]{1,0:T(8,128)(2,1)} %param.8), kind=kLoop, calls=%fused_computation.2 | loop fusion | flops 4717824 | bytes 3148800 | tf_op jit(solution)/shard_map/reduce_sum | solution.py:16
  5.4 0.0 copy-done.1
  5.4 1.1 copy.9
  6.6 0.0 copy-start
  6.6 0.0 copy-start.3
  6.6 2.6 %copy.10 = bf16[128,2816]{0,1:T(8,128)(2,1)} copy(f32[128,2816]{1,0:T(8,128)} %param.11) | data formatting | bytes 2162688 | tf_op args[3]
  9.2 0.0 copy-start.2
  9.2 2.7 %pad_maximum_fusion.gu_ref = bf16[2,2816,128]{2,1,0:T(8,128)(2,1)} fusion(bf16[1,2816,128]{2,1,0:T(8,128)(2,1)} %bitcast.12, bf16[1,2816,128]{2,1,0:T(8,128)(2,1)} %bitcast.11), kind=kLoop, calls=%fused_computation.5 | loop fusion | flops 720896 | bytes 2883584 | tf_op jit(solution)/shard_map/stack | solution.py:319
  11.9 0.0 copy-done.2
  11.9 0.9 convert_element_type.17.d_ref
  12.8 0.0 copy-done
  12.8 0.0 copy-done.3
  12.8 2.4 fusion.2.xn_ref
  15.3 227.1 %shard_map.82 = bf16[768,1024]{1,0:T(8,128)(2,1)} custom-call(bf16[2,2816,128]{2,1,0:T(8,128)(2,1)} %pad_maximum_fusion.gu_ref, bf16[2816,128]{1,0:T(8,128)(2,1)} %convert_element_type.17.d_ref, bf16[768,2048]{1,0:T(8,128)(2,1)} %fusion.2.xn_ref, f32[1,704]{1,0:T(1,128)} %broadcast_in_dim.11.gs_ref, f32[1,704]{1,0:T(1,128)} %broadcast_in_dim.12.us_ref, ...), custom_call_target="tpu_custom_call" | custom-call | tf_op jit(solution)/shard_map/pallas_call | solution.py:327
  242.4 2.7 %copy.12 = bf16[768,1024]{1,0:T(8,128)(2,1)} copy(bf16[768,1024]{1,0:T(8,128)(2,1)} %shard_map.82) | data formatting | bytes 3145728
  (1 shorter events, 0.0 us)
Async XLA Ops:
  0.0 5.4 %copy-start.1 = (f32[128,2816]{1,0:T(8,128)S(1)}, f32[128,2816]{1,0:T(8,128)}, u32[]{:S(2)}) copy-start(f32[128,2816]{1,0:T(8,128)} %param.10) | copy-start | bytes 4325380
  6.6 6.3 %copy-start = (bf16[768,2048]{1,0:T(8,128)(2,1)S(1)}, bf16[768,2048]{1,0:T(8,128)(2,1)}, u32[]{:S(2)}) copy-start(bf16[768,2048]{1,0:T(8,128)(2,1)} %param.8) | copy-start | bytes 9437188
  6.6 6.3 %copy-start.3 = (f32[2048]{0:T(1024)S(1)}, f32[2048]{0:T(1024)}, u32[]{:S(2)}) copy-start(f32[2048]{0:T(1024)} %param.9) | copy-start | bytes 24580
  9.2 2.7 %copy-start.2 = (f32[2816,128]{1,0:T(8,128)S(1)}, f32[2816,128]{1,0:T(8,128)}, u32[]{:S(2)}) copy-start(f32[2816,128]{1,0:T(8,128)} %param.14) | copy-start | bytes 4325380
